TPU v7x, 128 devices: a whole 4x4x4 slice. The times are simulated.
128 devices in a mesh: sp: 64 (over z, y, x), tp: 2 (over core).
Axes of the slice: x: 4, y: 4, z: 4, core: 2. Of those that a mesh axis runs over, the one named last changes fastest.
Arguments:
- queries: bfloat16 [8192, 1024], P('sp', 'tp'), may hold values from -6 to 6
- keys: bfloat16 [8192, 1024], P('sp', 'tp'), may hold values from -6 to 6
- values: bfloat16 [8192, 2048], P('sp', 'tp'), may hold values from -6 to 6
- out_gate: bfloat16 [8192, 2048], P('sp', 'tp'), may hold values from -6 to 6
- decay_rate: float32 [8], P('tp'), may hold values from 0 to 1
- residual: bfloat16 [8192, 2048], P(('sp', 'tp')), may hold values from -6 to 6
- out_weight: bfloat16 [2048, 2048], P('tp'), may hold values from -0.125 to 0.125
- ffn_gain: float32 [2048], replicated, may hold values from 0.1 to 1.9
- route_ids: int32 [8192, 4], P(('sp', 'tp')), may hold values from 0 to 63, all different within a row; in each aligned block of 64 rows (0 to 63, 64 to 127, ...) at most 8 rows name the same one
- route_weights: float32 [8192, 4], P(('sp', 'tp')), may hold values from 0.1 to 1
- gate_up: bfloat16 [64, 2048, 2048], P('sp', None, 'tp'), may hold values from -0.375 to 0.375
- lin_up: bfloat16 [64, 2048, 2048], P('sp', None, 'tp'), may hold values from -0.375 to 0.375
- down_weight: bfloat16 [64, 2048, 2048], P('sp', 'tp'), may hold values from -0.03125 to 0.03125
Outputs:
- layer_out: bfloat16 [8192, 2048], P(('sp', 'tp'))
Inputs may be any that keep to these rules, and one draw needn't show every extreme that they name: `route_ids`: within the rows of one device (aligned blocks of 64 rows), no expert is named by more than 8 entries, a bound that some block reaches; the 4 experts of a row differ.
All inputs are finite; a program needn't handle non-finite values.
Results may differ from a plain program's by a relative error of at most 0.03.
Values may be sent and summed in bfloat16 or wider, within the bound.
A program may use at most 128 MiB of HBM per device.

v0:
```python
import jax
import jax.numpy as jnp
from jax import lax
from jax.sharding import Mesh
from jax.sharding import PartitionSpec as P

D = 2048
DK = 128
DV = 256
SP = ("sp_0", "sp_1", "sp_2")
SP_TP = ("sp_0", "sp_1", "sp_2", "tp")
EPS = 1e-05
CLAMP_LIMIT = 7.0
SIGMOID_SLOPE = 1.702
TOP_PRECISION = lax.Precision.HIGHEST


def carried_state(state_delta, log_gamma, block_len):
    peers, mine = (lax.axis_size(SP), lax.axis_index(SP))
    heads = state_delta.shape[0]
    pieces = state_delta.astype(jnp.bfloat16).reshape(peers, -1)
    arrived = lax.all_to_all(pieces, SP, split_axis=0, concat_axis=0, tiled=True)
    own_log = lax.dynamic_index_in_dim(log_gamma, mine * heads // peers, keepdims=False)
    order = jnp.arange(peers, dtype=jnp.float32)
    gap = order[:, None] - 1.0 - order[None, :]
    weight = jnp.where(gap >= 0, jnp.exp(jnp.maximum(gap, 0.0) * block_len * own_log), 0.0)
    before = jnp.dot(weight, arrived.astype(jnp.float32), precision=TOP_PRECISION)
    returned = lax.all_to_all(
        before.astype(jnp.bfloat16), SP, split_axis=0, concat_axis=0, tiled=True
    )
    return returned.reshape(state_delta.shape).astype(jnp.float32)


def in_blocks(array, dim, peers):
    before, after = (array.shape[:dim], array.shape[dim + 1 :])
    return jnp.moveaxis(array.reshape(*before, peers, -1, *after), dim, 0)


def summed_on_arrival(array, axis, dim):
    tiles = in_blocks(array, dim, lax.axis_size(axis))
    arrived = lax.all_to_all(tiles, axis, split_axis=0, concat_axis=0, tiled=True)
    return arrived.astype(jnp.float32).sum(axis=0)


def expert_act(row_block, gate_part, lin_part):
    gate_pre = jnp.dot(row_block, gate_part, preferred_element_type=jnp.float32)
    lin_pre = jnp.dot(row_block, lin_part, preferred_element_type=jnp.float32)
    gate_clip = jnp.minimum(gate_pre, CLAMP_LIMIT)
    lin_clip = jnp.clip(lin_pre, -CLAMP_LIMIT, CLAMP_LIMIT)
    return (gate_clip * jax.nn.sigmoid(SIGMOID_SLOPE * gate_clip) * (lin_clip + 1.0)).astype(
        jnp.bfloat16
    )


def local(
    queries,
    keys,
    values,
    out_gate,
    decay_rate,
    residual,
    out_weight,
    ffn_gain,
    route_ids,
    route_weights,
    gate_up,
    lin_up,
    down_weight,
):
    block_len = queries.shape[0]
    local_heads = decay_rate.shape[0]
    log_gamma = -decay_rate
    query_heads = queries.astype(jnp.float32).reshape(block_len, local_heads, DK).transpose(1, 0, 2)
    per_head_keys = keys.astype(jnp.float32).reshape(block_len, local_heads, DK).transpose(
        1, 0, 2
    ) * DK ** (-0.5)
    per_head_values = (
        values.astype(jnp.float32).reshape(block_len, local_heads, DV).transpose(1, 0, 2)
    )
    positions = jnp.arange(block_len, dtype=jnp.float32)
    offsets = positions[:, None] - positions[None, :]
    causal = offsets >= 0
    decay_mask = jnp.where(
        causal[None], jnp.exp(jnp.where(causal, offsets, 0.0)[None] * log_gamma[:, None, None]), 0.0
    )
    trailing_decay = jnp.exp((block_len - 1.0 - positions)[None, :] * log_gamma[:, None])
    lead_decay = jnp.exp((positions + 1.0)[None, :] * log_gamma[:, None])
    attention_scores = (
        jnp.einsum("hqd,hkd->hqk", query_heads, per_head_keys, precision=TOP_PRECISION) * decay_mask
    )
    intra_block_term = jnp.einsum(
        "zfp,zpn->zfn", attention_scores, per_head_values, precision=TOP_PRECISION
    )
    state_delta = jnp.einsum(
        "mxs,mxq->msq",
        per_head_keys * trailing_decay[:, :, None],
        per_head_values,
        precision=TOP_PRECISION,
    )
    carried = carried_state(state_delta, log_gamma, block_len)
    cross_term = (
        jnp.einsum("hqd,hdv->hqv", query_heads, carried, precision=TOP_PRECISION)
        * lead_decay[:, :, None]
    )
    retained = intra_block_term + cross_term
    normed = retained * lax.rsqrt(jnp.mean(retained * retained, axis=-1, keepdims=True) + EPS)
    gated = (
        normed.transpose(1, 0, 2).reshape(block_len, local_heads * DV)
        * jax.nn.silu(out_gate.astype(jnp.float32))
    ).astype(jnp.bfloat16)
    mix_rows = summed_on_arrival(
        jnp.dot(gated, out_weight, preferred_element_type=jnp.float32).astype(jnp.bfloat16), "tp", 0
    )
    mixed = (residual.astype(jnp.float32) + mix_rows).astype(jnp.bfloat16)
    mixed_wide = mixed.astype(jnp.float32)
    normed_rows = (
        mixed_wide
        * lax.rsqrt(jnp.mean(mixed_wide * mixed_wide, axis=-1, keepdims=True) + EPS)
        * ffn_gain
    ).astype(jnp.bfloat16)
    experts = lax.axis_size(SP)
    own_rows = route_ids.shape[0]
    top_count = route_ids.shape[1]
    capacity = own_rows * top_count * lax.axis_size("tp") // experts
    flat_ids = route_ids.reshape(-1)
    one_hot = (flat_ids[:, None] == jnp.arange(experts, dtype=jnp.int32)[None, :]).astype(jnp.int32)
    slot_rank = jnp.sum(one_hot * (jnp.cumsum(one_hot, axis=0) - 1), axis=1)
    slot_index = flat_ids * capacity + slot_rank
    source_row = jnp.arange(own_rows * top_count, dtype=jnp.int32) // top_count
    slot_source = (
        jnp.full((experts * capacity,), own_rows, jnp.int32).at[slot_index].set(source_row)
    )
    padded = jnp.concatenate([normed_rows, jnp.zeros((1, D), jnp.bfloat16)], axis=0)
    outgoing = padded[slot_source].reshape(experts, capacity, D)
    gate_half = gate_up[0]
    lin_half = lin_up[0]
    down_half = down_weight[0]
    pair_rows = lax.all_gather(
        lax.all_to_all(outgoing, SP, split_axis=0, concat_axis=0, tiled=True),
        "tp",
        axis=0,
        tiled=True,
    )
    activation = expert_act(pair_rows.reshape(-1, D), gate_half, lin_half)
    partial_value = jnp.dot(activation, down_half, preferred_element_type=jnp.float32).reshape(
        pair_rows.shape
    )
    summed = summed_on_arrival(partial_value.astype(jnp.bfloat16), "tp", 0)
    returned = lax.all_to_all(
        summed.astype(jnp.bfloat16), SP, split_axis=0, concat_axis=0, tiled=True
    )
    picked = (
        returned.reshape(experts * capacity, D)[slot_index]
        .reshape(own_rows, top_count, D)
        .astype(jnp.float32)
    )
    expert_sum = jnp.sum(picked * route_weights[:, :, None], axis=1)
    return (mixed_wide + expert_sum).astype(jnp.bfloat16)


def solution(mesh):
    torus = Mesh(mesh.devices.reshape(4, 4, 4, mesh.shape["tp"]), ("sp_0", "sp_1", "sp_2", "tp"))
    in_specs = (
        P(SP, "tp"),
        P(SP, "tp"),
        P(SP, "tp"),
        P(SP, "tp"),
        P("tp"),
        P(SP_TP, None),
        P("tp", None),
        P(),
        P(SP_TP, None),
        P(SP_TP, None),
        P(SP, None, "tp"),
        P(SP, None, "tp"),
        P(SP, "tp", None),
    )
    out_specs = P(SP_TP, None)
    return jax.shard_map(local, mesh=torus, in_specs=in_specs, out_specs=out_specs, check_vma=False)
```

profile of v0, /device:TPU:0, one launch (start us, length us, event | category | flops | bytes accessed | tf_op | source)
XLA Modules:
  0.0 202.1 jit_solution(13798051839371577354)
XLA Ops:
  6.5 0.7 neg.10
  7.3 1.0 copy.102
  8.3 0.1 multiply_exponential_fusion
  8.3 1.3 convolution_convert_fusion.2
  9.7 0.1 all_to_all.35
  9.8 0.6 broadcast.223
  10.4 2.2 %reduce.4 = bf16[64,2048]{1,0:T(8,128)(2,1)S(1)} reduce(bf16[64,1,2048]{2,1,0:T(2,128)(2,1)S(1)} %all_to_all.35, bf16[]{:T(256)} %broadcast.223), dimensions={1}, to_apply=%all_to_all.35.reduce_sub_computation | reduce | bytes 524290 | tf_op jit(solution)/shard_map/all_to_all | solution.py:22
  12.6 0.9 reshape.247
  13.5 11.7 %all-to-all-start = ((bf16[64,2,1024]{2,1,0:T(2,128)(2,1)}), bf16[64,2,1024]{2,1,0:T(2,128)(2,1)S(1)}, u32[]{:S(2)}, u32[]{:S(2)}) async-start(bf16[64,2,1024]{2,1,0:T(2,128)(2,1)} %reshape.247), calls=%async_computation | async-start | bytes 524288 | tf_op jit(solution)/shard_map/all_to_all | solution.py:22
  25.2 0.1 multiply_exponential_fusion.1
  25.3 0.8 copy.90
  26.1 0.1 eq.29
  26.2 0.1 eq.25
  26.3 0.7 broadcast_multiply_fusion
  27.0 0.6 reduce-window.6
  27.6 0.2 slice_reduce_fusion
  27.8 0.1 copy.89
  27.9 0.1 mul.229
  28.0 0.1 fusion.49
  28.2 0.6 dynamic_slice.4
  29.3 1.4 scatter_custom_fusion
  30.8 5.0 %all-to-all-done = bf16[64,2,1024]{2,1,0:T(2,128)(2,1)S(1)} async-done(((bf16[64,2,1024]{2,1,0:T(2,128)(2,1)}), bf16[64,2,1024]{2,1,0:T(2,128)(2,1)S(1)}, u32[]{:S(2)}, u32[]{:S(2)}) %all-to-all-start) | async-done | bytes 262176 | tf_op jit(solution)/shard_map/all_to_all | solution.py:22
  35.8 0.2 reshape.248
  36.0 0.5 fusion.11
  36.5 0.8 reduce.5
  37.3 0.9 reshape.249
  38.2 5.4 %all-to-all-start.1 = ((bf16[64,2,1024]{2,1,0:T(2,128)(2,1)}), bf16[64,2,1024]{2,1,0:T(2,128)(2,1)S(1)}, u32[]{:S(2)}, u32[]{:S(2)}) async-start(bf16[64,2,1024]{2,1,0:T(2,128)(2,1)} %reshape.249), calls=%async_computation.1 | async-start | bytes 524288 | tf_op jit(solution)/shard_map/all_to_all | solution.py:28
  43.5 0.0 all-gather.2.cloned.1.call-start
  43.6 0.2 copy.88
  43.8 0.4 fusion.22
  44.2 10.0 %all-to-all-done.1 = bf16[64,2,1024]{2,1,0:T(2,128)(2,1)S(1)} async-done(((bf16[64,2,1024]{2,1,0:T(2,128)(2,1)}), bf16[64,2,1024]{2,1,0:T(2,128)(2,1)S(1)}, u32[]{:S(2)}, u32[]{:S(2)}) %all-to-all-start.1) | async-done | bytes 262176 | tf_op jit(solution)/shard_map/all_to_all | solution.py:28
  54.2 0.2 reshape.250
  54.4 1.5 reduce.1
  55.9 0.1 reshape.207
  56.0 0.2 fusion.43
  56.3 0.5 fusion.32
  56.8 0.2 fusion.34
  57.0 0.2 copy.87
  57.2 0.0 copy-start.3
  57.2 0.1 fusion.35
  57.4 2.9 %convolution_convert_fusion = bf16[128,2048]{1,0:T(8,128)(2,1)S(1)} fusion(bf16[128,1024]{0,1:T(8,128)(2,1)S(1)} %fusion.35, bf16[1024,2048]{1,0:T(8,128)(2,1)} %param.19), kind=kOutput, calls=%fused_computation.13 | convolution fusion | flops 537133056 | bytes 4980736 | tf_op jit(solution)/shard_map/dot_general | solution.py:112
  60.3 4.2 %all_to_all.42 = bf16[2,64,2048]{2,1,0:T(8,128)(2,1)S(1)} all-to-all(bf16[2,64,2048]{2,1,0:T(8,128)(2,1)S(1)} %bitcast.118), channel_id=1, replica_groups=mesh['sp_0'=4,'sp_1'=4,'sp_2'=4,'tp'=2] {'tp'}, dimensions={0} | all-to-all | bytes 1048576 | tf_op jit(solution)/shard_map/all_to_all | solution.py:41
  64.5 0.1 convert_reduce_fusion
  64.6 0.2 fusion.27
  64.8 0.1 fusion.29
  65.0 2.5 %gather_fusion = bf16[512,2048]{1,0:T(8,128)(2,1)S(1)} fusion(bf16[65,2048]{1,0:T(8,128)(2,1)S(1)} %concatenate.3, s32[1024]{0:T(1024)S(1)} %pad_clamp_fusion.1), kind=kCustom, calls=%fused_computation | custom fusion | bytes 4196352 | tf_op jit(solution)/shard_map/gather | solution.py:134
  67.4 35.2 %all_to_all.43 = bf16[64,8,2048]{2,1,0:T(8,128)(2,1)} all-to-all(bf16[64,8,2048]{2,1,0:T(8,128)(2,1)S(1)} %bitcast.114), channel_id=1, replica_groups=mesh['sp_0'=4,'sp_1'=4,'sp_2'=4,'tp'=2] {'sp_0','sp_1','sp_2'}, dimensions={0} | all-to-all | bytes 4194304 | tf_op jit(solution)/shard_map/all_to_all | solution.py:139
  102.7 0.0 all-gather.2.cloned.1.call-update
  102.7 13.1 %all-gather.2.cloned.1.call-done = bf16[128,8,2048]{2,1,0:T(8,128)(2,1)} async-done(((bf16[64,8,2048]{2,1,0:T(8,128)(2,1)}), bf16[128,8,2048]{2,1,0:T(8,128)(2,1)}) %all-gather.2.cloned.1.call-update) | async-done | bytes 4194320 | tf_op jit(solution)/shard_map/all_gather | solution.py:138
  115.8 7.6 %fusion.2 = f32[1024,1024]{1,0:T(8,128)S(1)} fusion(bf16[1,2048,1024]{2,1,0:T(8,128)(2,1)} %param.24, bf16[128,8,2048]{2,1,0:T(8,128)(2,1)} %all-gather.2.cloned.1.call-done), kind=kOutput, calls=%fused_computation.5 | convolution fusion | flops 4294967296 | bytes 12582912 | tf_op jit(solution)/shard_map/dot_general | solution.py:47
  123.5 5.8 %fusion.17 = bf16[128,8,1024]{2,1,0:T(8,128)(2,1)S(1)} fusion(f32[1024,1024]{1,0:T(8,128)S(1)} %fusion.2, bf16[1,2048,1024]{2,1,0:T(8,128)(2,1)S(1)} %copy-done.6, bf16[128,8,2048]{2,1,0:T(8,128)(2,1)S(1)} %copy-done.8), kind=kOutput, calls=%fused_computation.18 | convolution fusion | flops 4305453056 | bytes 14680064 | tf_op jit(solution)/shard_map/dot_general | solution.py:46
  129.3 5.2 %fusion.8 = bf16[128,8,2048]{2,0,1:T(8,128)(2,1)S(1)} fusion(bf16[1,1024,2048]{2,1,0:T(8,128)(2,1)S(1)} %copy-done.7, bf16[128,8,1024]{2,1,0:T(8,128)(2,1)S(1)} %fusion.17), kind=kOutput, calls=%fused_computation.12 | convolution fusion | flops 4297064448 | bytes 10485760 | tf_op jit(solution)/shard_map/dot_general | solution.py:145
  134.5 0.6 copy.94
  135.1 8.2 %all_to_all.44 = bf16[2,64,8,2048]{3,1,2,0:T(8,128)(2,1)} all-to-all(bf16[2,64,8,2048]{3,1,2,0:T(8,128)(2,1)S(1)} %copy.94), channel_id=1, replica_groups=mesh['sp_0'=4,'sp_1'=4,'sp_2'=4,'tp'=2] {'tp'}, dimensions={0} | all-to-all | bytes 8388608 | tf_op jit(solution)/shard_map/all_to_all | solution.py:41
  143.2 3.5 %reduce_sum.64 = bf16[64,8,2048]{2,0,1:T(8,128)(2,1)S(1)} reduce(bf16[2,64,8,2048]{3,1,2,0:T(8,128)(2,1)} %all_to_all.44, bf16[]{:T(256)} %constant.96.clone.1), dimensions={0}, to_apply=%region_7.8 | reduce | flops 1048576 | bytes 6291458 | tf_op jit(solution)/shard_map/reduce_sum | solution.py:42
  146.7 0.0 copy-start.5
  146.7 2.5 %copy.96 = bf16[64,8,2048]{2,1,0:T(8,128)(2,1)} copy(bf16[64,8,2048]{2,0,1:T(8,128)(2,1)S(1)} %reduce_sum.64) | data formatting | bytes 4194304 | tf_op jit(solution)/shard_map/reduce_sum | solution.py:42
  149.2 10.6 %all-to-all-start.5 = ((bf16[64,8,2048]{2,1,0:T(8,128)(2,1)}), bf16[64,8,2048]{2,1,0:T(8,128)(2,1)S(1)}, u32[]{:S(2)}, u32[]{:S(2)}) async-start(bf16[64,8,2048]{2,1,0:T(8,128)(2,1)} %copy.96), calls=%async_computation.5 | async-start | bytes 4194304 | tf_op jit(solution)/shard_map/all_to_all | solution.py:149
  159.9 0.7 copy.97
  160.6 29.4 %all-to-all-done.5 = bf16[64,8,2048]{2,1,0:T(8,128)(2,1)S(1)} async-done(((bf16[64,8,2048]{2,1,0:T(8,128)(2,1)}), bf16[64,8,2048]{2,1,0:T(8,128)(2,1)S(1)}, u32[]{:S(2)}, u32[]{:S(2)}) %all-to-all-start.5) | async-done | bytes 2097184 | tf_op jit(solution)/shard_map/all_to_all | solution.py:149
  190.0 1.4 gather_fusion.1
  191.4 0.7 reshape.215
  192.1 2.4 %multiply_reduce_fusion = f32[64,2048]{1,0:T(8,128)S(1)} fusion(f32[64,4,2048]{2,1,0:T(4,128)S(1)} %reshape.215, f32[64,4]{1,0:T(8,128)} %copy.97), kind=kLoop, calls=%fused_computation.17 | loop fusion | flops 917504 | bytes 2622464 | tf_op jit(solution)/shard_map/reduce_sum | solution.py:157
  194.5 0.8 fusion.30
  (31 shorter events, 0.2 us)
Async XLA Ops:
  6.5 37.3 %copy-start = (bf16[128,512]{1,0:T(8,128)(2,1)S(1)}, bf16[128,512]{1,0:T(8,128)(2,1)}, u32[]{:S(2)}) copy-start(bf16[128,512]{1,0:T(8,128)(2,1)} %param.13) | copy-start | bytes 393220
  6.5 37.1 %copy-start.2 = (bf16[128,1024]{1,0:T(8,128)(2,1)S(1)}, bf16[128,1024]{1,0:T(8,128)(2,1)}, u32[]{:S(2)}) copy-start(bf16[128,1024]{1,0:T(8,128)(2,1)} %param.16) | copy-start | bytes 786436
  13.5 42.8 %copy-start.1 = (bf16[128,1024]{1,0:T(8,128)(2,1)S(1)}, bf16[128,1024]{1,0:T(8,128)(2,1)}, u32[]{:S(2)}) copy-start(bf16[128,1024]{1,0:T(8,128)(2,1)} %param.15) | copy-start | bytes 786436
  13.5 22.3 %all-to-all-start = ((bf16[64,2,1024]{2,1,0:T(2,128)(2,1)}), bf16[64,2,1024]{2,1,0:T(2,128)(2,1)S(1)}, u32[]{:S(2)}, u32[]{:S(2)}) async-start(bf16[64,2,1024]{2,1,0:T(2,128)(2,1)} %reshape.247), calls=%async_computation | async-start | bytes 524288 | tf_op jit(solution)/shard_map/all_to_all | solution.py:22
  38.2 16.0 %all-to-all-start.1 = ((bf16[64,2,1024]{2,1,0:T(2,128)(2,1)}), bf16[64,2,1024]{2,1,0:T(2,128)(2,1)S(1)}, u32[]{:S(2)}, u32[]{:S(2)}) async-start(bf16[64,2,1024]{2,1,0:T(2,128)(2,1)} %reshape.249), calls=%async_computation.1 | async-start | bytes 524288 | tf_op jit(solution)/shard_map/all_to_all | solution.py:28
  43.5 72.3 %all-gather.2.cloned.1.call-start = ((), (), s32[]{:S(2)}) async-start(), calls=%async_computation.6 | async-start | bytes 6291456 | tf_op jit(solution)/shard_map/all_gather | solution.py:138
  57.2 7.4 %copy-start.3 = (bf16[64,2048]{1,0:T(8,128)(2,1)S(1)}, bf16[64,2048]{1,0:T(8,128)(2,1)}, u32[]{:S(2)}) copy-start(bf16[64,2048]{1,0:T(8,128)(2,1)} %param.18) | copy-start | bytes 786436
  57.4 7.4 %copy-start.4 = (f32[2048]{0:T(1024)S(1)}, f32[2048]{0:T(1024)}, u32[]{:S(2)}) copy-start(f32[2048]{0:T(1024)} %param.20) | copy-start | bytes 24580
  115.8 7.7 %copy-start.6 = (bf16[1,2048,1024]{2,1,0:T(8,128)(2,1)S(1)}, bf16[1,2048,1024]{2,1,0:T(8,128)(2,1)}, u32[]{:S(2)}) copy-start(bf16[1,2048,1024]{2,1,0:T(8,128)(2,1)} %param.23) | copy-start | bytes 12582916
  115.8 7.7 %copy-start.8 = (bf16[128,8,2048]{2,1,0:T(8,128)(2,1)S(1)}, bf16[128,8,2048]{2,1,0:T(8,128)(2,1)}, u32[]{:S(2)}) copy-start(bf16[128,8,2048]{2,1,0:T(8,128)(2,1)} %all-gather.2.cloned.1.call-done) | copy-start | bytes 12582916
  123.5 5.8 %copy-start.7 = (bf16[1,1024,2048]{2,1,0:T(8,128)(2,1)S(1)}, bf16[1,1024,2048]{2,1,0:T(8,128)(2,1)}, u32[]{:S(2)}) copy-start(bf16[1,1024,2048]{2,1,0:T(8,128)(2,1)} %param.25) | copy-start | bytes 12582916
  146.7 13.1 %copy-start.5 = (f32[64,4]{0,1:T(4,128)S(1)}, f32[64,4]{0,1:T(4,128)}, u32[]{:S(2)}) copy-start(f32[64,4]{0,1:T(4,128)} %param.22) | copy-start | bytes 3076
  149.2 40.8 %all-to-all-start.5 = ((bf16[64,8,2048]{2,1,0:T(8,128)(2,1)}), bf16[64,8,2048]{2,1,0:T(8,128)(2,1)S(1)}, u32[]{:S(2)}, u32[]{:S(2)}) async-start(bf16[64,8,2048]{2,1,0:T(8,128)(2,1)} %copy.96), calls=%async_computation.5 | async-start | bytes 4194304 | tf_op jit(solution)/shard_map/all_to_all | solution.py:149
Sparse Core Ops, SparseCore 0:
  102.8 12.9 all-gather.1
where the time goes:
time: 203 us; the launch traced here: 202 us
  waiting for transfers between devices  57.5 us (28%)
  blocking collectives  47.6 us (23%)
  starting transfers between devices  27.7 us (14%)
  matrix products  24.4 us (12%)
  local copies, waits for them, and re-layouts  16.2 us (8%)
  between operations  14.4 us (7%)
  other arithmetic  14.3 us (7%)
    all_to_all x1, blocking collectives, local(): lax.all_to_all(outgoing, SP, split_axis=0, concat_axis=0, tiled=True)  35.2 us
    all_to_all x1, waiting for transfers between devices, local(): lax.all_to_all(summed.astype(jnp.bfloat16), SP, split_axis=0, concat_axis...  29.4 us
    all_gather x1, waiting for transfers between devices, local(): lax.all_gather(lax.all_to_all(outgoing, SP, split_axis=0, concat_axis=0,...  13.1 us
    all_to_all x2, blocking collectives, summed_on_arrival(): lax.all_to_all(tiles, axis, split_axis=0, concat_axis=0, tiled=True)  12.3 us
    all_to_all x1, starting transfers between devices, carried_state(): lax.all_to_all(pieces, SP, split_axis=0, concat_axis=0, tiled=True)  11.7 us
    all_to_all x1, starting transfers between devices, local(): lax.all_to_all(summed.astype(jnp.bfloat16), SP, split_axis=0, concat_axis...  10.6 us
    all_to_all x1, waiting for transfers between devices, carried_state(): lax.all_to_all(before.astype(jnp.bfloat16), SP, split_axis=0, concat_axis...  9.95 us
    dot_general x1, matrix products, expert_act(): lin_pre = jnp.dot(row_block, lin_part, preferred_element_type=jnp.float32)  7.65 us
  transfers between devices with their start and end apart: 4, of which 4 were waited for; matrix products, arithmetic and copies ran while one was open for 3% of the time, Pallas kernels for 0%

commit v1 on v0

--- a/solution.py
+++ b/solution.py
@@ -135,12 +135,17 @@
     gate_half = gate_up[0]
     lin_half = lin_up[0]
     down_half = down_weight[0]
-    pair_rows = lax.all_gather(
-        lax.all_to_all(outgoing, SP, split_axis=0, concat_axis=0, tiled=True),
-        "tp",
-        axis=0,
-        tiled=True,
-    )
+
+    def set_check(tile_in, in_dim=0):
+        axis_id = "tp"
+        axis_total = lax.axis_size(axis_id)
+        entries = []
+        for at in range(tile_in.ndim):
+            entries.append(axis_total if at == in_dim else 1)
+        value_now = jnp.tile(tile_in, entries)
+        return lax.all_to_all(value_now, axis_id, tiled=True, concat_axis=in_dim, split_axis=in_dim)
+
+    pair_rows = set_check(lax.all_to_all(outgoing, SP, split_axis=0, concat_axis=0, tiled=True))
     activation = expert_act(pair_rows.reshape(-1, D), gate_half, lin_half)
     partial_value = jnp.dot(activation, down_half, preferred_element_type=jnp.float32).reshape(
         pair_rows.shape

time: 203 us -> 176 us (0.87)
  between operations: 14.4 us -> 1.02 us
  waiting for transfers between devices: 57.5 us -> 44.8 us
  blocking collectives: 47.6 us -> 54.8 us
  starting transfers between devices: 27.7 us -> 22.7 us
  matrix products: 24.4 us -> 21.4 us
    all_gather x1 -> x0, waiting for transfers between devices: 13.1 us -> none  [local(): lax.all_gather(lax.all_to_all(outgoing, SP, split_axis=0, concat_axis=0,...]
    all_to_all x0 -> x1, blocking collectives: none -> 7.37 us  [set_check(): lax.all_to_all(value_now, axis_id, tiled=True, concat_axis=in_dim, split_...]
    all_to_all x1, starting transfers between devices: 10.6 us -> 5.68 us  [local(): lax.all_to_all(summed.astype(jnp.bfloat16), SP, split_axis=0, concat_axis...]
    dot_general x1, matrix products: 7.65 us -> 4.54 us  [expert_act(): lin_pre = jnp.dot(row_block, lin_part, preferred_element_type=jnp.float32)]
  transfers between devices with their start and end apart: 4 -> 3, of which waited for: 4 -> 3; matrix products, arithmetic and copies ran while one was open for 3% -> 4% of each run, Pallas kernels for 0% -> 0%
where the time goes in v1:
time: 176 us
  blocking collectives  54.8 us (31%)
  waiting for transfers between devices  44.8 us (25%)
  starting transfers between devices  22.7 us (13%)
  matrix products  21.4 us (12%)
  local copies, waits for them, and re-layouts  16.7 us (9%)
  other arithmetic  14.2 us (8%)
    all_to_all x1, blocking collectives, local(): lax.all_to_all(outgoing, SP, split_axis=0, concat_axis=0, tiled=True)  35.1 us
    all_to_all x1, waiting for transfers between devices, local(): lax.all_to_all(summed.astype(jnp.bfloat16), SP, split_axis=0, concat_axis...  29.8 us
    all_to_all x2, blocking collectives, summed_on_arrival(): lax.all_to_all(tiles, axis, split_axis=0, concat_axis=0, tiled=True)  12.3 us
    all_to_all x1, starting transfers between devices, carried_state(): lax.all_to_all(pieces, SP, split_axis=0, concat_axis=0, tiled=True)  11.7 us
    all_to_all x1, waiting for transfers between devices, carried_state(): lax.all_to_all(before.astype(jnp.bfloat16), SP, split_axis=0, concat_axis...  10 us
    all_to_all x1, blocking collectives, set_check(): lax.all_to_all(value_now, axis_id, tiled=True, concat_axis=in_dim, split_...  7.37 us
    dot_general x1, matrix products, expert_act(): gate_pre = jnp.dot(row_block, gate_part, preferred_element_type=jnp.float32)  5.77 us
    all_to_all x1, starting transfers between devices, local(): lax.all_to_all(summed.astype(jnp.bfloat16), SP, split_axis=0, concat_axis...  5.68 us
  transfers between devices with their start and end apart: 3, of which 3 were waited for; matrix products, arithmetic and copies ran while one was open for 4% of the time, Pallas kernels for 0%

profile of v1, /device:TPU:0, one launch (start us, length us, event | category | flops | bytes accessed | tf_op | source)
XLA Modules:
  0.0 175.6 jit_solution(7799539435737695797)
XLA Ops:
  0.0 0.7 neg.10
  0.7 1.0 copy.102
  1.7 0.1 multiply_exponential_fusion
  1.8 1.3 convolution_convert_fusion.2
  3.1 0.1 all_to_all.39
  3.3 0.6 broadcast.226
  3.9 2.2 %reduce.4 = bf16[64,2048]{1,0:T(8,128)(2,1)S(1)} reduce(bf16[64,1,2048]{2,1,0:T(2,128)(2,1)S(1)} %all_to_all.39, bf16[]{:T(256)} %broadcast.226), dimensions={1}, to_apply=%all_to_all.39.reduce_sub_computation | reduce | bytes 524290 | tf_op jit(solution)/shard_map/all_to_all | solution.py:22
  6.1 0.9 reshape.251
  7.0 11.7 %all-to-all-start = ((bf16[64,2,1024]{2,1,0:T(2,128)(2,1)}), bf16[64,2,1024]{2,1,0:T(2,128)(2,1)S(1)}, u32[]{:S(2)}, u32[]{:S(2)}) async-start(bf16[64,2,1024]{2,1,0:T(2,128)(2,1)} %reshape.251), calls=%async_computation | async-start | bytes 524288 | tf_op jit(solution)/shard_map/all_to_all | solution.py:22
  18.7 0.1 multiply_exponential_fusion.1
  18.8 0.8 copy.90
  19.5 0.1 eq.29
  19.6 0.1 eq.25
  19.8 0.7 broadcast_multiply_fusion
  20.5 0.6 reduce-window.6
  21.1 0.2 slice_reduce_fusion
  21.3 0.1 copy.89
  21.4 0.1 mul.229
  21.5 0.1 fusion.49
  21.7 0.6 dynamic_slice.4
  22.8 1.4 scatter_custom_fusion
  24.2 5.0 %all-to-all-done = bf16[64,2,1024]{2,1,0:T(2,128)(2,1)S(1)} async-done(((bf16[64,2,1024]{2,1,0:T(2,128)(2,1)}), bf16[64,2,1024]{2,1,0:T(2,128)(2,1)S(1)}, u32[]{:S(2)}, u32[]{:S(2)}) %all-to-all-start) | async-done | bytes 262176 | tf_op jit(solution)/shard_map/all_to_all | solution.py:22
  29.2 0.2 reshape.252
  29.5 0.5 fusion.11
  29.9 0.8 reduce.5
  30.8 0.9 reshape.253
  31.6 5.4 %all-to-all-start.1 = ((bf16[64,2,1024]{2,1,0:T(2,128)(2,1)}), bf16[64,2,1024]{2,1,0:T(2,128)(2,1)S(1)}, u32[]{:S(2)}, u32[]{:S(2)}) async-start(bf16[64,2,1024]{2,1,0:T(2,128)(2,1)} %reshape.253), calls=%async_computation.1 | async-start | bytes 524288 | tf_op jit(solution)/shard_map/all_to_all | solution.py:28
  37.0 0.2 copy.88
  37.2 0.4 fusion.22
  37.6 10.0 %all-to-all-done.1 = bf16[64,2,1024]{2,1,0:T(2,128)(2,1)S(1)} async-done(((bf16[64,2,1024]{2,1,0:T(2,128)(2,1)}), bf16[64,2,1024]{2,1,0:T(2,128)(2,1)S(1)}, u32[]{:S(2)}, u32[]{:S(2)}) %all-to-all-start.1) | async-done | bytes 262176 | tf_op jit(solution)/shard_map/all_to_all | solution.py:28
  47.6 0.2 reshape.254
  47.8 1.5 reduce.1
  49.4 0.1 reshape.211
  49.5 0.2 fusion.43
  49.7 0.5 fusion.32
  50.3 0.2 fusion.34
  50.5 0.2 copy.87
  50.7 0.0 copy-start.4
  50.7 0.1 fusion.35
  50.9 0.0 copy-start.5
  50.9 2.9 %convolution_convert_fusion = bf16[128,2048]{1,0:T(8,128)(2,1)S(1)} fusion(bf16[128,1024]{0,1:T(8,128)(2,1)S(1)} %fusion.35, bf16[1024,2048]{1,0:T(8,128)(2,1)} %param.19), kind=kOutput, calls=%fused_computation.13 | convolution fusion | flops 537133056 | bytes 4980736 | tf_op jit(solution)/shard_map/dot_general | solution.py:112
  53.8 4.2 %all_to_all.47 = bf16[2,64,2048]{2,1,0:T(8,128)(2,1)S(1)} all-to-all(bf16[2,64,2048]{2,1,0:T(8,128)(2,1)S(1)} %bitcast.120), channel_id=1, replica_groups=mesh['sp_0'=4,'sp_1'=4,'sp_2'=4,'tp'=2] {'tp'}, dimensions={0} | all-to-all | bytes 1048576 | tf_op jit(solution)/shard_map/all_to_all | solution.py:41
  58.0 0.1 convert_reduce_fusion
  58.1 0.2 fusion.27
  58.3 0.1 fusion.29
  58.4 2.5 %gather_fusion = bf16[512,2048]{1,0:T(8,128)(2,1)S(1)} fusion(bf16[65,2048]{1,0:T(8,128)(2,1)S(1)} %concatenate.3, s32[1024]{0:T(1024)S(1)} %pad_clamp_fusion.1), kind=kCustom, calls=%fused_computation | custom fusion | bytes 4196352 | tf_op jit(solution)/shard_map/gather | solution.py:134
  60.9 35.1 %all_to_all.48 = bf16[64,8,2048]{2,1,0:T(8,128)(2,1)S(1)} all-to-all(bf16[64,8,2048]{2,1,0:T(8,128)(2,1)S(1)} %bitcast.116), channel_id=1, replica_groups=mesh['sp_0'=4,'sp_1'=4,'sp_2'=4,'tp'=2] {'sp_0','sp_1','sp_2'}, dimensions={0} | all-to-all | bytes 4194304 | tf_op jit(solution)/shard_map/all_to_all | solution.py:148
  96.0 0.5 tile.4
  96.6 0.0 copy-start.7
  96.6 7.4 %all_to_all.49 = bf16[128,8,2048]{2,1,0:T(8,128)(2,1)S(1)} all-to-all(bf16[128,8,2048]{2,1,0:T(8,128)(2,1)S(1)} %bitcast.115), channel_id=1, replica_groups=mesh['sp_0'=4,'sp_1'=4,'sp_2'=4,'tp'=2] {'tp'}, dimensions={0} | all-to-all | bytes 8388608 | tf_op jit(solution)/shard_map/all_to_all | solution.py:146
  103.9 4.5 %fusion.2 = f32[1024,1024]{1,0:T(8,128)S(1)} fusion(bf16[1,2048,1024]{2,1,0:T(8,128)(2,1)S(1)} %copy-done.7, bf16[128,8,2048]{2,1,0:T(8,128)(2,1)S(1)} %all_to_all.49), kind=kOutput, calls=%fused_computation.5 | convolution fusion | flops 4294967296 | bytes 12582912 | tf_op jit(solution)/shard_map/dot_general | solution.py:47
  108.5 5.8 %fusion.17 = bf16[128,8,1024]{2,1,0:T(8,128)(2,1)S(1)} fusion(f32[1024,1024]{1,0:T(8,128)S(1)} %fusion.2, bf16[1,2048,1024]{2,1,0:T(8,128)(2,1)S(1)} %copy-done.8, bf16[128,8,2048]{2,1,0:T(8,128)(2,1)S(1)} %all_to_all.49), kind=kOutput, calls=%fused_computation.18 | convolution fusion | flops 4305453056 | bytes 14680064 | tf_op jit(solution)/shard_map/dot_general | solution.py:46
  114.3 5.2 %fusion.8 = bf16[128,8,2048]{2,0,1:T(8,128)(2,1)S(1)} fusion(bf16[1,1024,2048]{2,1,0:T(8,128)(2,1)S(1)} %copy-done.9, bf16[128,8,1024]{2,1,0:T(8,128)(2,1)S(1)} %fusion.17), kind=kOutput, calls=%fused_computation.12 | convolution fusion | flops 4297064448 | bytes 10485760 | tf_op jit(solution)/shard_map/dot_general | solution.py:150
  119.5 0.6 copy.94
  120.1 8.2 %all_to_all.50 = bf16[2,64,8,2048]{3,1,2,0:T(8,128)(2,1)} all-to-all(bf16[2,64,8,2048]{3,1,2,0:T(8,128)(2,1)S(1)} %copy.94), channel_id=1, replica_groups=mesh['sp_0'=4,'sp_1'=4,'sp_2'=4,'tp'=2] {'tp'}, dimensions={0} | all-to-all | bytes 8388608 | tf_op jit(solution)/shard_map/all_to_all | solution.py:41
  128.3 3.5 %reduce_sum.64 = bf16[64,8,2048]{2,0,1:T(8,128)(2,1)S(1)} reduce(bf16[2,64,8,2048]{3,1,2,0:T(8,128)(2,1)} %all_to_all.50, bf16[]{:T(256)} %constant.96.clone.1), dimensions={0}, to_apply=%region_7.8 | reduce | flops 1048576 | bytes 6291458 | tf_op jit(solution)/shard_map/reduce_sum | solution.py:42
  131.8 2.5 %copy.96 = bf16[64,8,2048]{2,1,0:T(8,128)(2,1)} copy(bf16[64,8,2048]{2,0,1:T(8,128)(2,1)S(1)} %reduce_sum.64) | data formatting | bytes 4194304 | tf_op jit(solution)/shard_map/reduce_sum | solution.py:42
  134.3 5.7 %all-to-all-start.6 = ((bf16[64,8,2048]{2,1,0:T(8,128)(2,1)}), bf16[64,8,2048]{2,1,0:T(8,128)(2,1)S(1)}, u32[]{:S(2)}, u32[]{:S(2)}) async-start(bf16[64,8,2048]{2,1,0:T(8,128)(2,1)} %copy.96), calls=%async_computation.6 | async-start | bytes 4194304 | tf_op jit(solution)/shard_map/all_to_all | solution.py:154
  140.0 0.7 copy.97
  140.7 29.8 %all-to-all-done.6 = bf16[64,8,2048]{2,1,0:T(8,128)(2,1)S(1)} async-done(((bf16[64,8,2048]{2,1,0:T(8,128)(2,1)}), bf16[64,8,2048]{2,1,0:T(8,128)(2,1)S(1)}, u32[]{:S(2)}, u32[]{:S(2)}) %all-to-all-start.6) | async-done | bytes 2097184 | tf_op jit(solution)/shard_map/all_to_all | solution.py:154
  170.4 1.4 gather_fusion.1
  171.8 0.7 reshape.219
  172.5 2.3 %multiply_reduce_fusion = f32[64,2048]{1,0:T(8,128)S(1)} fusion(f32[64,4,2048]{2,1,0:T(4,128)S(1)} %reshape.219, f32[64,4]{1,0:T(8,128)} %copy.97), kind=kLoop, calls=%fused_computation.17 | loop fusion | flops 917504 | bytes 2622464 | tf_op jit(solution)/shard_map/reduce_sum | solution.py:162
  174.8 0.8 fusion.30
  (32 shorter events, 0.2 us)
Async XLA Ops:
  0.0 37.2 %copy-start = (bf16[128,512]{1,0:T(8,128)(2,1)S(1)}, bf16[128,512]{1,0:T(8,128)(2,1)}, u32[]{:S(2)}) copy-start(bf16[128,512]{1,0:T(8,128)(2,1)} %param.13) | copy-start | bytes 393220
  0.0 37.0 %copy-start.3 = (bf16[128,1024]{1,0:T(8,128)(2,1)S(1)}, bf16[128,1024]{1,0:T(8,128)(2,1)}, u32[]{:S(2)}) copy-start(bf16[128,1024]{1,0:T(8,128)(2,1)} %param.16) | copy-start | bytes 786436
  7.0 42.8 %copy-start.2 = (bf16[128,1024]{1,0:T(8,128)(2,1)S(1)}, bf16[128,1024]{1,0:T(8,128)(2,1)}, u32[]{:S(2)}) copy-start(bf16[128,1024]{1,0:T(8,128)(2,1)} %param.15) | copy-start | bytes 786436
  7.0 22.3 %all-to-all-start = ((bf16[64,2,1024]{2,1,0:T(2,128)(2,1)}), bf16[64,2,1024]{2,1,0:T(2,128)(2,1)S(1)}, u32[]{:S(2)}, u32[]{:S(2)}) async-start(bf16[64,2,1024]{2,1,0:T(2,128)(2,1)} %reshape.251), calls=%async_computation | async-start | bytes 524288 | tf_op jit(solution)/shard_map/all_to_all | solution.py:22
  31.6 16.0 %all-to-all-start.1 = ((bf16[64,2,1024]{2,1,0:T(2,128)(2,1)}), bf16[64,2,1024]{2,1,0:T(2,128)(2,1)S(1)}, u32[]{:S(2)}, u32[]{:S(2)}) async-start(bf16[64,2,1024]{2,1,0:T(2,128)(2,1)} %reshape.253), calls=%async_computation.1 | async-start | bytes 524288 | tf_op jit(solution)/shard_map/all_to_all | solution.py:28
  50.7 7.4 %copy-start.4 = (bf16[64,2048]{1,0:T(8,128)(2,1)S(1)}, bf16[64,2048]{1,0:T(8,128)(2,1)}, u32[]{:S(2)}) copy-start(bf16[64,2048]{1,0:T(8,128)(2,1)} %param.18) | copy-start | bytes 786436
  50.9 7.4 %copy-start.5 = (f32[2048]{0:T(1024)S(1)}, f32[2048]{0:T(1024)}, u32[]{:S(2)}) copy-start(f32[2048]{0:T(1024)} %param.20) | copy-start | bytes 24580
  96.6 7.4 %copy-start.7 = (bf16[1,2048,1024]{2,1,0:T(8,128)(2,1)S(1)}, bf16[1,2048,1024]{2,1,0:T(8,128)(2,1)}, u32[]{:S(2)}) copy-start(bf16[1,2048,1024]{2,1,0:T(8,128)(2,1)} %param.24) | copy-start | bytes 12582916
  103.9 4.5 %copy-start.8 = (bf16[1,2048,1024]{2,1,0:T(8,128)(2,1)S(1)}, bf16[1,2048,1024]{2,1,0:T(8,128)(2,1)}, u32[]{:S(2)}) copy-start(bf16[1,2048,1024]{2,1,0:T(8,128)(2,1)} %param.23) | copy-start | bytes 12582916
  108.5 5.8 %copy-start.9 = (bf16[1,1024,2048]{2,1,0:T(8,128)(2,1)S(1)}, bf16[1,1024,2048]{2,1,0:T(8,128)(2,1)}, u32[]{:S(2)}) copy-start(bf16[1,1024,2048]{2,1,0:T(8,128)(2,1)} %param.25) | copy-start | bytes 12582916
  131.7 8.2 %copy-start.6 = (f32[64,4]{0,1:T(4,128)S(1)}, f32[64,4]{0,1:T(4,128)}, u32[]{:S(2)}) copy-start(f32[64,4]{0,1:T(4,128)} %param.22) | copy-start | bytes 3076
  134.3 36.2 %all-to-all-start.6 = ((bf16[64,8,2048]{2,1,0:T(8,128)(2,1)}), bf16[64,8,2048]{2,1,0:T(8,128)(2,1)S(1)}, u32[]{:S(2)}, u32[]{:S(2)}) async-start(bf16[64,8,2048]{2,1,0:T(8,128)(2,1)} %copy.96), calls=%async_computation.6 | async-start | bytes 4194304 | tf_op jit(solution)/shard_map/all_to_all | solution.py:154
  170.4 5.2 %copy-start.1 = (bf16[128,512]{1,0:T(8,128)(2,1)S(1)}, bf16[128,512]{1,0:T(8,128)(2,1)}, u32[]{:S(2)}) copy-start(bf16[128,512]{1,0:T(8,128)(2,1)} %param.13) | copy-start | bytes 393220
